TPU v7x, 512 devices: a 8x2x16 block of a 8x8x16 slice. The times are simulated.
512 devices in a mesh: grp: 2 (over y), ep: 32 (over z, core), tp: 8 (over x).
Axes of the slice: x: 8, y: 2, z: 16, core: 2. Of those that a mesh axis runs over, the one named last changes fastest.
The devices are a block of a 8x8x16 slice.
Arguments:
- tokens: bfloat16 [16384, 2048], P(('grp', 'ep'), 'tp'), parts along dimension 0, may hold values from -6 to 6
- norm_gain: float32 [2048], replicated, may hold values from 0.1 to 1.9
- expert_ids: int32 [16384, 2], P(('grp', 'ep')), parts along dimension 0, may hold values from 0 to 31, all different within a row; in each aligned block of 256 rows (0 to 255, 256 to 511, ...) at most 24 rows name the same one
- gate_weights: float32 [16384, 2], P(('grp', 'ep')), parts along dimension 0, may hold values from 0.25 to 1
- w_gate: bfloat16 [32, 2048, 3072], P('ep', None, 'tp'), may hold values from -0.125 to 0.125
- w_up: bfloat16 [32, 2048, 3072], P('ep', None, 'tp'), may hold values from -0.125 to 0.125
- w_down: bfloat16 [32, 3072, 2048], P('ep', 'tp'), may hold values from -0.15625 to 0.15625
Outputs:
- mixed: bfloat16 [16384, 2048], P(('grp', 'ep'), 'tp'), parts along dimension 0
There are 2 independent parts, one for each index of `grp`. A program takes and returns all parts, laid end to end along the dimension named above; an argument that names none is the same for every part. Nothing has to cross between parts.
Inputs may be any that keep to these rules, and one draw needn't show every extreme that they name: `expert_ids`: each token names 2 different experts. Within the 256 rows of one index of ep (aligned blocks) no expert is named more than 24 times, and in some blocks one expert is named exactly 24 times.
All inputs are finite; a program needn't handle non-finite values.
Results may differ from a plain program's by a relative error of at most 0.015.
Values may be sent and summed in bfloat16 or wider, within the bound.
A program may use at most 64 MiB of HBM per device.

v0:
```python
import jax
import jax.numpy as jnp
from jax import lax
from jax.sharding import Mesh
from jax.sharding import PartitionSpec as P

EP = ("ep_0", "ep_1")
GRP_EP = ("grp", "ep_0", "ep_1")
epsilon = 1e-06


def sent_to_all(array, axis):
    count = lax.axis_size(axis)
    return lax.all_to_all(
        jnp.broadcast_to(array[None], (count, *array.shape)), axis, 0, 0, tiled=True
    )


def over_copies(array, axis):
    everything = sent_to_all(array, axis)
    return jnp.sum(everything, axis=0)


def in_blocks(array, dim, count):
    dims = array.shape
    blocks = array.reshape(*dims[:dim], count, dims[dim] // count, *dims[dim + 1 :])
    return jnp.moveaxis(blocks, dim, 0)


def joined_along(blocks, dim):
    dims = list(blocks.shape[1:])
    dims[dim] *= blocks.shape[0]
    return jnp.moveaxis(blocks, 0, dim).reshape(dims)


def moved_by_axis(blocks, axes, order):
    inside = blocks.shape[1:]
    whole = blocks.reshape(*(lax.axis_size(a) for a in axes), *inside)
    for k in order:
        whole = lax.all_to_all(whole, axes[k], k, k, tiled=True)
    return whole.reshape(-1, *inside)


def core_and_chips(array, groups, order, split_dim, concat_dim):
    count = lax.axis_size(groups[0]) * lax.axis_size(groups[1])
    blocks = in_blocks(array, split_dim, count)
    return joined_along(moved_by_axis(blocks, groups, order), concat_dim)


def on_device(tokens, norm_gain, expert_ids, gate_weights, w_gate, w_up, w_down):
    tok_count = tokens.shape[0]
    top_count = expert_ids.shape[1]
    expert_count = lax.axis_size(EP)
    capacity = 3 * tok_count * top_count // (2 * expert_count)
    model_width = norm_gain.shape[0]
    flat_ids = expert_ids.reshape(-1)
    onehot = (flat_ids[:, None] == jnp.arange(expert_count, dtype=jnp.int32)[None, :]).astype(
        jnp.int32
    )
    earlier = jnp.cumsum(onehot, axis=0) - onehot
    slot_index = jnp.sum(earlier * onehot, axis=1)
    dest_index = flat_ids * capacity + slot_index
    owner_index = jnp.arange(tok_count * top_count, dtype=jnp.int32) // top_count
    slot_token = (
        jnp.full((expert_count * capacity,), tok_count, jnp.int32).at[dest_index].set(owner_index)
    )
    tok_values = tokens.astype(jnp.float32)
    square_sum = over_copies(jnp.sum(tok_values * tok_values, axis=1, keepdims=True), "tp")
    col_count = tokens.shape[1]
    gain_part = lax.dynamic_slice_in_dim(norm_gain, lax.axis_index("tp") * col_count, col_count)
    normed = (tok_values * lax.rsqrt(square_sum / model_width + epsilon) * gain_part).astype(
        jnp.bfloat16
    )
    buffer = jnp.take(normed, slot_token, axis=0, mode="fill", fill_value=0).reshape(
        expert_count, capacity, -1
    )
    received = core_and_chips(buffer, ("ep_0", "ep_1"), (1, 0), 0, 0)
    source_count, item_count, col_count = received.shape
    tok_rows = received.reshape(-1, col_count)
    col_piece = lax.all_gather(tok_rows, "tp", axis=1, tiled=True)
    gate_rows = w_gate[0]
    up_rows = w_up[0]
    gate_part = jnp.dot(col_piece, gate_rows, preferred_element_type=jnp.float32)
    up_part = jnp.dot(col_piece, up_rows, preferred_element_type=jnp.float32)
    hidden = (jax.nn.silu(gate_part) * up_part).astype(jnp.bfloat16)
    partial_value = jnp.dot(hidden, w_down[0], preferred_element_type=jnp.float32)
    partial_value = partial_value.reshape(source_count, item_count, -1)
    summed = lax.psum_scatter(
        partial_value.astype(jnp.bfloat16), "tp", scatter_dimension=2, tiled=True
    )
    came_back = lax.all_to_all(summed, EP, split_axis=0, concat_axis=0, tiled=True)
    picked = came_back.reshape(expert_count * capacity, -1)[dest_index].astype(jnp.float32)
    weighted = picked * gate_weights.reshape(-1)[:, None]
    return jnp.sum(weighted.reshape(tok_count, top_count, -1), axis=1).astype(jnp.bfloat16)


def solution(mesh):
    finer = Mesh(
        mesh.devices.reshape(mesh.shape["grp"], 16, 2, mesh.shape["tp"]),
        ("grp", "ep_0", "ep_1", "tp"),
    )
    in_specs = (
        P(GRP_EP, "tp"),
        P(),
        P(GRP_EP, None),
        P(GRP_EP, None),
        P(EP, None, "tp"),
        P(EP, None, "tp"),
        P(EP, "tp", None),
    )
    out_specs = P(GRP_EP, "tp")
    return jax.shard_map(
        on_device, mesh=finer, in_specs=in_specs, out_specs=out_specs, check_vma=False
    )
```

profile of v0, /device:TPU:65, one launch (start us, length us, event | category | flops | bytes accessed | tf_op | source)
XLA Modules:
  0.0 271.2 jit_solution(14151282188558710371)
XLA Ops:
  6.5 0.0 copy-start
  6.6 1.1 fusion.11
  7.7 0.6 broadcast_in_dim.29
  8.3 7.9 %all-to-all-start = ((f32[8,256,1]{1,2,0:T(1,128)}), f32[8,256,1]{1,2,0:T(1,128)S(1)}, u32[]{:S(2)}, u32[]{:S(2)}) async-start(f32[8,256,1]{1,2,0:T(1,128)} %broadcast_in_dim.29), calls=%async_computation | async-start | bytes 16384 | tf_op jit(solution)/shard_map/all_to_all | solution.py:14
  16.2 0.1 all-gather.2.cloned.1.call-start
  16.2 0.8 copy.15
  17.0 0.1 eq.29
  17.2 0.1 eq.25
  17.3 0.7 broadcast_multiply_fusion
  18.0 1.2 reduce-window.6
  19.2 0.2 slice_reduce_fusion
  19.5 0.1 copy.14
  19.6 0.1 mul.59
  19.8 0.1 fusion.16
  19.9 2.4 scatter_custom_fusion
  22.4 0.1 broadcast_in_dim.27
  22.5 0.8 dynamic_slice.3
  23.3 0.0 all-to-all-done
  23.3 1.0 fusion.13
  24.3 2.7 gather_fusion
  27.0 0.2 copy_select_fusion
  27.1 0.0 copy-start.3
  27.2 41.3 %all_to_all.20 = bf16[16,2,1,24,256]{4,3,0,2,1:T(8,128)(2,1)S(1)} all-to-all(bf16[16,2,1,24,256]{4,3,0,2,1:T(8,128)(2,1)S(1)} %copy_select_fusion), channel_id=1, replica_groups=mesh['grp'=2,'ep_0'=16,'ep_1'=2,'tp'=8] {'ep_1'}, dimensions={1} | all-to-all | bytes 786432 | tf_op jit(solution)/shard_map/all_to_all | solution.py:40
  68.5 24.6 %all_to_all.21 = bf16[16,2,1,24,256]{4,3,1,2,0:T(8,128)(2,1)} all-to-all(bf16[16,2,1,24,256]{4,3,1,2,0:T(8,128)(2,1)S(1)} %copy.20), channel_id=1, replica_groups=mesh['grp'=2,'ep_0'=16,'ep_1'=2,'tp'=8] {'ep_0'}, dimensions={0} | all-to-all | bytes 786432 | tf_op jit(solution)/shard_map/all_to_all | solution.py:40
  93.1 0.1 all-gather.2.cloned.1.call-update
  93.2 0.1 reduce-scatter.2.cloned.1.call-start
  93.3 59.5 %all-gather.2.cloned.1.call-done = bf16[768,2048]{1,0:T(8,128)(2,1)} async-done(((bf16[768,256]{1,0:T(8,128)(2,1)}), bf16[768,2048]{1,0:T(8,128)(2,1)}) %all-gather.2.cloned.1.call-update) | async-done | bytes 3145744 | tf_op jit(solution)/shard_map/all_gather | solution.py:80
  152.8 0.0 copy-done.3
  152.8 0.0 copy-start.2
  152.8 0.0 copy-start.4
  152.8 3.8 %fusion.3 = f32[768,384]{1,0:T(8,128)S(1)} fusion(bf16[768,2048]{1,0:T(8,128)(2,1)} %all-gather.2.cloned.1.call-done, bf16[1,2048,384]{2,1,0:T(8,128)(2,1)S(1)} %copy-done.3), kind=kOutput, calls=%fused_computation.7 | convolution fusion | flops 1207959552 | bytes 5898240 | tf_op jit(solution)/shard_map/dot_general | solution.py:83
  156.6 0.0 copy-done.2
  156.6 0.0 copy-done.4
  156.6 1.8 fusion.8
  158.5 0.0 copy-done
  158.5 3.5 %convolution_convert_fusion = bf16[32,24,2048]{2,1,0:T(8,128)(2,1)} fusion(bf16[32,24,384]{2,1,0:T(8,128)(2,1)S(1)} %bitcast.48, bf16[1,384,2048]{2,1,0:T(8,128)(2,1)S(1)} %copy-done), kind=kOutput, calls=%fused_computation.3 | convolution fusion | flops 1209532416 | bytes 5308416 | tf_op jit(solution)/shard_map/dot_general | solution.py:86
  162.0 0.0 copy-start.1
  162.0 0.1 reduce-scatter.2.cloned.1.call-update
  162.0 54.2 %reduce-scatter.2.cloned.1.call-done = bf16[32,24,256]{2,1,0:T(8,128)(2,1)} async-done(((bf16[32,24,2048]{2,1,0:T(8,128)(2,1)}), bf16[32,24,256]{2,1,0:T(8,128)(2,1)}) %reduce-scatter.2.cloned.1.call-update) | async-done | bytes 393232 | tf_op jit(solution)/shard_map/reduce_scatter | solution.py:88
  216.2 16.9 %all-to-all-start.3 = ((bf16[32,24,256]{2,1,0:T(8,128)(2,1)}), bf16[32,24,256]{2,1,0:T(8,128)(2,1)S(1)}, u32[]{:S(2)}, u32[]{:S(2)}) async-start(bf16[32,24,256]{2,1,0:T(8,128)(2,1)} %reduce-scatter.2.cloned.1.call-done), calls=%async_computation.4 | async-start | bytes 786432 | tf_op jit(solution)/shard_map/all_to_all | solution.py:91
  233.2 0.0 copy-done.1
  233.2 0.1 copy.21
  233.3 27.4 %all-to-all-done.3 = bf16[32,24,256]{2,1,0:T(8,128)(2,1)S(1)} async-done(((bf16[32,24,256]{2,1,0:T(8,128)(2,1)}), bf16[32,24,256]{2,1,0:T(8,128)(2,1)S(1)}, u32[]{:S(2)}, u32[]{:S(2)}) %all-to-all-start.3) | async-done | bytes 393248 | tf_op jit(solution)/shard_map/all_to_all | solution.py:91
  260.7 1.9 gather_fusion.1
  262.7 0.3 reshape.98
  262.9 1.4 multiply_reduce_fusion
  (13 shorter events, 0.2 us)
Async XLA Ops:
  6.5 152.0 %copy-start = (bf16[1,384,2048]{2,1,0:T(8,128)(2,1)S(1)}, bf16[1,384,2048]{2,1,0:T(8,128)(2,1)}, u32[]{:S(2)}) copy-start(bf16[1,384,2048]{2,1,0:T(8,128)(2,1)} %param.13) | copy-start | bytes 4718596
  8.3 15.0 %all-to-all-start = ((f32[8,256,1]{1,2,0:T(1,128)}), f32[8,256,1]{1,2,0:T(1,128)S(1)}, u32[]{:S(2)}, u32[]{:S(2)}) async-start(f32[8,256,1]{1,2,0:T(1,128)} %broadcast_in_dim.29), calls=%async_computation | async-start | bytes 16384 | tf_op jit(solution)/shard_map/all_to_all | solution.py:14
  16.2 136.6 %all-gather.2.cloned.1.call-start = ((), (), s32[]{:S(2)}) async-start(), calls=%async_computation.5 | async-start | bytes 3538944 | tf_op jit(solution)/shard_map/all_gather | solution.py:80
  27.1 125.6 %copy-start.3 = (bf16[1,2048,384]{2,1,0:T(8,128)(2,1)S(1)}, bf16[1,2048,384]{2,1,0:T(8,128)(2,1)}, u32[]{:S(2)}) copy-start(bf16[1,2048,384]{2,1,0:T(8,128)(2,1)} %param.11) | copy-start | bytes 4718596
  93.2 123.0 %reduce-scatter.2.cloned.1.call-start = ((), (), s32[]{:S(2)}) async-start(), calls=%async_computation.6 | async-start | bytes 3538944 | tf_op jit(solution)/shard_map/reduce_scatter | solution.py:88
  152.8 3.8 %copy-start.2 = (bf16[768,2048]{1,0:T(8,128)(2,1)S(1)}, bf16[768,2048]{1,0:T(8,128)(2,1)}, u32[]{:S(2)}) copy-start(bf16[768,2048]{1,0:T(8,128)(2,1)} %all-gather.2.cloned.1.call-done) | copy-start | bytes 9437188
  152.8 3.8 %copy-start.4 = (bf16[1,2048,384]{2,1,0:T(8,128)(2,1)S(1)}, bf16[1,2048,384]{2,1,0:T(8,128)(2,1)}, u32[]{:S(2)}) copy-start(bf16[1,2048,384]{2,1,0:T(8,128)(2,1)} %param.12) | copy-start | bytes 4718596
  162.0 71.2 %copy-start.1 = (f32[256,2]{0,1:T(2,128)S(1)}, f32[256,2]{0,1:T(2,128)}, u32[]{:S(2)}) copy-start(f32[256,2]{0,1:T(2,128)} %param.10) | copy-start | bytes 6148
  216.2 44.5 %all-to-all-start.3 = ((bf16[32,24,256]{2,1,0:T(8,128)(2,1)}), bf16[32,24,256]{2,1,0:T(8,128)(2,1)S(1)}, u32[]{:S(2)}, u32[]{:S(2)}) async-start(bf16[32,24,256]{2,1,0:T(8,128)(2,1)} %reduce-scatter.2.cloned.1.call-done), calls=%async_computation.4 | async-start | bytes 786432 | tf_op jit(solution)/shard_map/all_to_all | solution.py:91
Sparse Core Ops, SparseCore 0:
  93.3 59.4 all-gather.1
  162.2 54.0 reduce-scatter.1
where the time goes:
time: 272 us; the launch traced here: 271 us
  waiting for transfers between devices  141 us (52%)
  blocking collectives  65.9 us (24%)
  starting transfers between devices  24.9 us (9%)
  between operations  13.6 us (5%)
  local copies, waits for them, and re-layouts  10.6 us (4%)
  matrix products  9.14 us (3%)
  other arithmetic  5.77 us (2%)
    all_to_all x2, blocking collectives, moved_by_axis(): whole = lax.all_to_all(whole, axes[k], k, k, tiled=True)  65.9 us
    all_gather x1, waiting for transfers between devices, on_device(): col_piece = lax.all_gather(tok_rows, 'tp', axis=1, tiled=True)  59.5 us
    reduce_scatter x1, waiting for transfers between devices, on_device(): lax.psum_scatter(partial_value.astype(jnp.bfloat16), 'tp', scatter_dimens...  54.2 us
    all_to_all x1, waiting for transfers between devices, on_device(): lax.all_to_all(summed, EP, split_axis=0, concat_axis=0, tiled=True)  27.4 us
    all_to_all x1, starting transfers between devices, on_device(): lax.all_to_all(summed, EP, split_axis=0, concat_axis=0, tiled=True)  16.9 us
    all_to_all x1, starting transfers between devices, sent_to_all(): lax.all_to_all(jnp.broadcast_to(array[None], (count, *array.shape)), axis...  7.86 us
  transfers between devices with their start and end apart: 4, of which 3 were waited for; matrix products, arithmetic and copies ran while one was open for 3% of the time, Pallas kernels for 0%

commit v1 on v0

--- a/solution.py
+++ b/solution.py
@@ -77,7 +77,7 @@
     received = core_and_chips(buffer, ("ep_0", "ep_1"), (1, 0), 0, 0)
     source_count, item_count, col_count = received.shape
     tok_rows = received.reshape(-1, col_count)
-    col_piece = lax.all_gather(tok_rows, "tp", axis=1, tiled=True)
+    col_piece = jnp.concatenate(lax.all_gather(tok_rows, axis_name="tp"), 1)
     gate_rows = w_gate[0]
     up_rows = w_up[0]
     gate_part = jnp.dot(col_piece, gate_rows, preferred_element_type=jnp.float32)

time: 272 us -> 265 us (0.974)
  waiting for transfers between devices: 141 us -> 130 us
  local copies, waits for them, and re-layouts: 10.6 us -> 15.3 us
    all_gather x1, waiting for transfers between devices: 59.5 us -> 52.5 us  [on_device(): col_piece = jnp.concatenate(lax.all_gather(tok_rows, axis_name='tp'), 1)]
    all_gather x0 -> x1, local copies, waits for them, and re-layouts: none -> 4.69 us  [on_device(): col_piece = jnp.concatenate(lax.all_gather(tok_rows, axis_name='tp'), 1)]
    reduce_scatter x1, waiting for transfers between devices: 54.2 us -> 50.3 us  [on_device(): lax.psum_scatter(partial_value.astype(jnp.bfloat16), 'tp', scatter_dimens...]
where the time goes in v1:
time: 265 us
  waiting for transfers between devices  130 us (49%)
  blocking collectives  65.8 us (25%)
  starting transfers between devices  24.9 us (9%)
  local copies, waits for them, and re-layouts  15.3 us (6%)
  between operations  13.6 us (5%)
  matrix products  9.2 us (3%)
  other arithmetic  5.77 us (2%)
    all_to_all x2, blocking collectives, moved_by_axis(): whole = lax.all_to_all(whole, axes[k], k, k, tiled=True)  65.8 us
    all_gather x1, waiting for transfers between devices, on_device(): col_piece = jnp.concatenate(lax.all_gather(tok_rows, axis_name='tp'), 1)  52.5 us
    reduce_scatter x1, waiting for transfers between devices, on_device(): lax.psum_scatter(partial_value.astype(jnp.bfloat16), 'tp', scatter_dimens...  50.3 us
    all_to_all x1, waiting for transfers between devices, on_device(): lax.all_to_all(summed, EP, split_axis=0, concat_axis=0, tiled=True)  27.4 us
    all_to_all x1, starting transfers between devices, on_device(): lax.all_to_all(summed, EP, split_axis=0, concat_axis=0, tiled=True)  16.9 us
    all_to_all x1, starting transfers between devices, sent_to_all(): lax.all_to_all(jnp.broadcast_to(array[None], (count, *array.shape)), axis...  7.86 us
  transfers between devices with their start and end apart: 4, of which 3 were waited for; matrix products, arithmetic and copies ran while one was open for 3% of the time, Pallas kernels for 0%

profile of v1, /device:TPU:65, one launch (start us, length us, event | category | flops | bytes accessed | tf_op | source)
XLA Modules:
  0.0 264.8 jit_solution(1449462710661547251)
XLA Ops:
  6.5 0.0 copy-start
  6.6 1.1 fusion.11
  7.7 0.6 broadcast_in_dim.29
  8.3 7.9 %all-to-all-start = ((f32[8,256,1]{1,2,0:T(1,128)}), f32[8,256,1]{1,2,0:T(1,128)S(1)}, u32[]{:S(2)}, u32[]{:S(2)}) async-start(f32[8,256,1]{1,2,0:T(1,128)} %broadcast_in_dim.29), calls=%async_computation | async-start | bytes 16384 | tf_op jit(solution)/shard_map/all_to_all | solution.py:14
  16.2 0.1 all-gather.2.cloned.1.call-start
  16.2 0.8 copy.22
  17.0 0.1 eq.29
  17.2 0.1 eq.25
  17.3 0.7 broadcast_multiply_fusion
  18.0 1.2 reduce-window.6
  19.2 0.2 slice_reduce_fusion
  19.5 0.1 copy.21
  19.6 0.1 mul.59
  19.8 0.1 fusion.16
  19.9 2.4 scatter_custom_fusion
  22.4 0.1 broadcast_in_dim.27
  22.5 0.8 dynamic_slice.3
  23.3 0.0 all-to-all-done
  23.3 1.0 fusion.13
  24.3 2.7 %gather_fusion = bf16[768,256]{1,0:T(8,128)(2,1)S(1)} fusion(bf16[256,256]{1,0:T(8,128)(2,1)S(1)} %fusion.13, s32[1024]{0:T(1024)S(1)} %pad_clamp_fusion.1), kind=kCustom, calls=%fused_computation | custom fusion | bytes 789504 | tf_op jit(solution)/shard_map/jit(_take)/gather | solution.py:74
  27.0 0.2 copy_select_fusion
  27.1 41.2 %all_to_all.20 = bf16[16,2,1,24,256]{4,3,0,2,1:T(8,128)(2,1)S(1)} all-to-all(bf16[16,2,1,24,256]{4,3,0,2,1:T(8,128)(2,1)S(1)} %copy_select_fusion), channel_id=1, replica_groups=mesh['grp'=2,'ep_0'=16,'ep_1'=2,'tp'=8] {'ep_1'}, dimensions={1} | all-to-all | bytes 786432 | tf_op jit(solution)/shard_map/all_to_all | solution.py:40
  68.4 24.6 %all_to_all.21 = bf16[16,2,1,24,256]{4,3,1,2,0:T(8,128)(2,1)} all-to-all(bf16[16,2,1,24,256]{4,3,1,2,0:T(8,128)(2,1)S(1)} %copy.27), channel_id=1, replica_groups=mesh['grp'=2,'ep_0'=16,'ep_1'=2,'tp'=8] {'ep_0'}, dimensions={0} | all-to-all | bytes 786432 | tf_op jit(solution)/shard_map/all_to_all | solution.py:40
  93.0 0.1 all-gather.2.cloned.1.call-update
  93.0 0.0 copy-start.2
  93.1 0.1 reduce-scatter.2.cloned.1.call-start
  93.1 52.5 %all-gather.2.cloned.1.call-done = bf16[8,768,256]{2,1,0:T(8,128)(2,1)} async-done(((bf16[1,768,256]{2,1,0:T(8,128)(2,1)}), bf16[8,768,256]{2,1,0:T(8,128)(2,1)}) %all-gather.2.cloned.1.call-update) | async-done | bytes 3145744 | tf_op jit(solution)/shard_map/all_gather | solution.py:80
  145.6 4.7 %copy.28 = bf16[8,768,256]{1,2,0:T(8,128)(2,1)} copy(bf16[8,768,256]{2,1,0:T(8,128)(2,1)} %all-gather.2.cloned.1.call-done) | data formatting | bytes 6291456 | tf_op jit(solution)/shard_map/all_gather | solution.py:80
  150.3 0.0 copy-done.2
  150.3 0.0 copy-start.1
  150.3 0.0 copy-start.4
  150.3 3.8 %fusion.3 = f32[768,384]{1,0:T(8,128)S(1)} fusion(bf16[768,2048]{0,1:T(8,128)(2,1)} %bitcast.46, bf16[1,2048,384]{2,1,0:T(8,128)(2,1)S(1)} %copy-done.2), kind=kOutput, calls=%fused_computation.7 | convolution fusion | flops 1207959552 | bytes 5898240 | tf_op jit(solution)/shard_map/dot_general | solution.py:83
  154.1 0.0 copy-done.1
  154.2 0.0 copy-done.4
  154.2 1.9 fusion.8
  156.0 0.0 copy-done
  156.1 3.5 %convolution_convert_fusion = bf16[32,24,2048]{2,1,0:T(8,128)(2,1)} fusion(bf16[32,24,384]{2,1,0:T(8,128)(2,1)S(1)} %bitcast.53, bf16[1,384,2048]{2,1,0:T(8,128)(2,1)S(1)} %copy-done), kind=kOutput, calls=%fused_computation.3 | convolution fusion | flops 1209532416 | bytes 5308416 | tf_op jit(solution)/shard_map/dot_general | solution.py:86
  159.5 0.0 copy-start.3
  159.5 0.1 reduce-scatter.2.cloned.1.call-update
  159.6 50.3 %reduce-scatter.2.cloned.1.call-done = bf16[32,24,256]{2,1,0:T(8,128)(2,1)} async-done(((bf16[32,24,2048]{2,1,0:T(8,128)(2,1)}), bf16[32,24,256]{2,1,0:T(8,128)(2,1)}) %reduce-scatter.2.cloned.1.call-update) | async-done | bytes 393232 | tf_op jit(solution)/shard_map/reduce_scatter | solution.py:88
  209.9 16.9 %all-to-all-start.3 = ((bf16[32,24,256]{2,1,0:T(8,128)(2,1)}), bf16[32,24,256]{2,1,0:T(8,128)(2,1)S(1)}, u32[]{:S(2)}, u32[]{:S(2)}) async-start(bf16[32,24,256]{2,1,0:T(8,128)(2,1)} %reduce-scatter.2.cloned.1.call-done), calls=%async_computation.4 | async-start | bytes 786432 | tf_op jit(solution)/shard_map/all_to_all | solution.py:91
  226.8 0.0 copy-done.3
  226.8 0.1 copy.29
  227.0 27.4 %all-to-all-done.3 = bf16[32,24,256]{2,1,0:T(8,128)(2,1)S(1)} async-done(((bf16[32,24,256]{2,1,0:T(8,128)(2,1)}), bf16[32,24,256]{2,1,0:T(8,128)(2,1)S(1)}, u32[]{:S(2)}, u32[]{:S(2)}) %all-to-all-start.3) | async-done | bytes 393248 | tf_op jit(solution)/shard_map/all_to_all | solution.py:91
  254.4 1.9 gather_fusion.1
  256.3 0.3 reshape.106
  256.6 1.4 multiply_reduce_fusion
  (13 shorter events, 0.2 us)
Async XLA Ops:
  6.5 149.5 %copy-start = (bf16[1,384,2048]{2,1,0:T(8,128)(2,1)S(1)}, bf16[1,384,2048]{2,1,0:T(8,128)(2,1)}, u32[]{:S(2)}) copy-start(bf16[1,384,2048]{2,1,0:T(8,128)(2,1)} %param.13) | copy-start | bytes 4718596
  8.3 15.0 %all-to-all-start = ((f32[8,256,1]{1,2,0:T(1,128)}), f32[8,256,1]{1,2,0:T(1,128)S(1)}, u32[]{:S(2)}, u32[]{:S(2)}) async-start(f32[8,256,1]{1,2,0:T(1,128)} %broadcast_in_dim.29), calls=%async_computation | async-start | bytes 16384 | tf_op jit(solution)/shard_map/all_to_all | solution.py:14
  16.2 129.4 %all-gather.2.cloned.1.call-start = ((), (), s32[]{:S(2)}) async-start(), calls=%async_computation.5 | async-start | bytes 3538944 | tf_op jit(solution)/shard_map/all_gather | solution.py:80
  93.0 57.2 %copy-start.2 = (bf16[1,2048,384]{2,1,0:T(8,128)(2,1)S(1)}, bf16[1,2048,384]{2,1,0:T(8,128)(2,1)}, u32[]{:S(2)}) copy-start(bf16[1,2048,384]{2,1,0:T(8,128)(2,1)} %param.11) | copy-start | bytes 4718596
  93.1 116.9 %reduce-scatter.2.cloned.1.call-start = ((), (), s32[]{:S(2)}) async-start(), calls=%async_computation.6 | async-start | bytes 3538944 | tf_op jit(solution)/shard_map/reduce_scatter | solution.py:88
  150.3 3.9 %copy-start.1 = (bf16[8,768,256]{1,2,0:T(8,128)(2,1)S(1)}, bf16[8,768,256]{1,2,0:T(8,128)(2,1)}, u32[]{:S(2)}) copy-start(bf16[8,768,256]{1,2,0:T(8,128)(2,1)} %copy.28) | copy-start | bytes 9437188
  150.3 3.9 %copy-start.4 = (bf16[1,2048,384]{2,1,0:T(8,128)(2,1)S(1)}, bf16[1,2048,384]{2,1,0:T(8,128)(2,1)}, u32[]{:S(2)}) copy-start(bf16[1,2048,384]{2,1,0:T(8,128)(2,1)} %param.12) | copy-start | bytes 4718596
  159.5 67.3 %copy-start.3 = (f32[256,2]{0,1:T(2,128)S(1)}, f32[256,2]{0,1:T(2,128)}, u32[]{:S(2)}) copy-start(f32[256,2]{0,1:T(2,128)} %param.10) | copy-start | bytes 6148
  209.9 44.4 %all-to-all-start.3 = ((bf16[32,24,256]{2,1,0:T(8,128)(2,1)}), bf16[32,24,256]{2,1,0:T(8,128)(2,1)S(1)}, u32[]{:S(2)}, u32[]{:S(2)}) async-start(bf16[32,24,256]{2,1,0:T(8,128)(2,1)} %reduce-scatter.2.cloned.1.call-done), calls=%async_computation.4 | async-start | bytes 786432 | tf_op jit(solution)/shard_map/all_to_all | solution.py:91
Sparse Core Ops, SparseCore 0:
  93.2 52.3 all-gather.1
  159.7 50.1 reduce-scatter.1
